TPU v7x, 32 devices: a whole 2x2x4 slice. The times are simulated.
32 devices in a mesh: rep: 2 (over x), fs: 8 (over z, y), tp: 2 (over core).
Axes of the slice: x: 2, y: 2, z: 4, core: 2. Of those that a mesh axis runs over, the one named last changes fastest.
Arguments:
- tokens: bfloat16 [4096, 2048], P(('rep', 'fs', 'tp')), may hold values from -6 to 6
- mix_gain: float32 [2048], replicated, may hold values from 0.1 to 1.9
- conv_in_weight: bfloat16 [2048, 1024], P('fs', 'tp'), may hold values from -0.125 to 0.125
- gate_outer_weight: bfloat16 [2048, 1024], P('fs', 'tp'), may hold values from -0.125 to 0.125
- gate_inner_weight: bfloat16 [2048, 1024], P('fs', 'tp'), may hold values from -0.125 to 0.125
- conv_taps: float32 [3, 1024], P(None, 'tp'), may hold values from -3.5 to 3.5
- out_weight: bfloat16 [1024, 2048], P('tp', 'fs'), may hold values from -0.1875 to 0.1875
- ff_gain: float32 [2048], replicated, may hold values from 0.1 to 1.9
- up_weight: bfloat16 [2048, 8192], P('fs', 'tp'), may hold values from -0.125 to 0.125
- down_weight: bfloat16 [8192, 2048], P('tp', 'fs'), may hold values from -0.0625 to 0.0625
Outputs:
- layer_out: bfloat16 [4096, 2048], P(('rep', 'fs', 'tp'))
All inputs are finite; a program needn't handle non-finite values.
Results may differ from a plain program's by a relative error of at most 0.023.
Values may be sent and summed in bfloat16 or wider, within the bound.
A program may use at most 128 MiB of HBM per device.

v0:
```python
import jax
import jax.numpy as jnp
from jax import lax
from jax.sharding import PartitionSpec as P

eps = 1e-06


def rms_scale(values, gain):
    widened = values.astype(jnp.float32)
    inverse = lax.rsqrt(jnp.mean(widened * widened, axis=-1, keepdims=True) + eps)
    return (widened * inverse * gain).astype(jnp.bfloat16)


def on_device(
    tokens,
    mix_gain,
    conv_in_weight,
    gate_outer_weight,
    gate_inner_weight,
    conv_taps,
    out_weight,
    ff_gain,
    up_weight,
    down_weight,
):
    normed = rms_scale(tokens, mix_gain)
    gathered = lax.all_gather(normed, "tp", axis=0, tiled=True)
    seq_rows = gathered.shape[0]
    segment = (
        lax.all_gather(conv_in_weight, "fs", axis=0, tiled=True),
        lax.all_gather(gate_outer_weight, "fs", axis=0, tiled=True),
        lax.all_gather(gate_inner_weight, "fs", axis=0, tiled=True),
    )
    conv_input, gate_outer, gate_inner = tuple(
        (jnp.dot(gathered, weight, preferred_element_type=jnp.float32) for weight in segment)
    )
    conv_input = conv_input.astype(jnp.bfloat16)
    gate_outer = gate_outer.astype(jnp.bfloat16)
    gate_inner = gate_inner.astype(jnp.bfloat16)
    gated = gate_inner.astype(jnp.float32) * conv_input.astype(jnp.float32)
    padded = jnp.pad(gated, ((2, 0), (0, 0)))
    convolved = (
        conv_taps[0] * padded[0:seq_rows]
        + conv_taps[1] * padded[1 : seq_rows + 1]
        + conv_taps[2] * padded[2 : seq_rows + 2]
    )
    mixed = (gate_outer.astype(jnp.float32) * convolved).astype(jnp.bfloat16)
    out_full = lax.all_gather(out_weight, "fs", axis=1, tiled=True)
    lefts = mixed
    mix_total = lax.psum_scatter(
        jnp.dot(lefts, out_full, preferred_element_type=jnp.float32).astype(jnp.bfloat16),
        "tp",
        scatter_dimension=0,
        tiled=True,
    ).astype(jnp.float32)
    resid = (tokens.astype(jnp.float32) + mix_total).astype(jnp.bfloat16)
    normed_ff = rms_scale(resid, ff_gain)
    ff_gathered = lax.all_gather(normed_ff, "tp", axis=0, tiled=True)
    up_full = lax.all_gather(up_weight, "fs", axis=0, tiled=True)
    preact = jnp.dot(ff_gathered, up_full, preferred_element_type=jnp.float32)
    hidden = jnp.square(jax.nn.relu(preact)).astype(jnp.bfloat16)
    down_full = lax.all_gather(down_weight, "fs", axis=1, tiled=True)
    lefts = hidden
    ff_total = lax.psum_scatter(
        jnp.dot(lefts, down_full, preferred_element_type=jnp.float32).astype(jnp.bfloat16),
        "tp",
        scatter_dimension=0,
        tiled=True,
    ).astype(jnp.float32)
    return (resid.astype(jnp.float32) + ff_total).astype(jnp.bfloat16)


def solution(mesh):
    in_specs = (
        P(("rep", "fs", "tp"), None),
        P(),
        P("fs", "tp"),
        P("fs", "tp"),
        P("fs", "tp"),
        P(None, "tp"),
        P("tp", "fs"),
        P(),
        P("fs", "tp"),
        P("tp", "fs"),
    )
    out_specs = P(("rep", "fs", "tp"), None)
    return jax.shard_map(
        on_device, mesh=mesh, in_specs=in_specs, out_specs=out_specs, check_vma=False
    )
```

profile of v0, /device:TPU:0, one launch (start us, length us, event | category | flops | bytes accessed | tf_op | source)
XLA Modules:
  0.0 740.0 jit_solution(13610082769893983982)
XLA Ops:
  6.5 0.0 copy-start.4
  6.5 0.0 all-gather.9.cloned.1.call-start
  6.5 1.2 fusion.8
  7.8 2.0 fusion.10
  9.8 0.0 all-gather.9.cloned.1.call-update
  9.8 0.0 all-gather.15.cloned.1.call-start
  9.9 0.7 all-gather.15.cloned.1.call-update
  10.6 0.0 all-gather.13.cloned.1.call-start
  10.6 0.7 all-gather.13.cloned.1.call-update
  11.3 0.0 all-gather.11.cloned.1.call-start
  11.4 0.5 all-gather.11.cloned.1.call-update
  11.9 0.0 all-gather.17.cloned.1.call-start
  12.0 0.5 all-gather.17.cloned.1.call-update
  12.5 0.0 reduce-scatter.3.cloned.1.call-start
  12.5 0.0 copy-done.4
  12.6 9.2 %all-gather.9.cloned.1.call-done = bf16[256,2048]{1,0:T(8,128)(2,1)} async-done(((bf16[128,2048]{1,0:T(8,128)(2,1)}), bf16[256,2048]{1,0:T(8,128)(2,1)}) %all-gather.9.cloned.1.call-update) | async-done | bytes 1048592 | tf_op jit(solution)/shard_map/all_gather | solution.py:28
  21.7 0.0 copy-start.2
  21.7 52.4 %all-gather.15.cloned.1.call-done = bf16[2048,512]{1,0:T(8,128)(2,1)} async-done(((bf16[256,512]{1,0:T(8,128)(2,1)}), bf16[2048,512]{1,0:T(8,128)(2,1)}) %all-gather.15.cloned.1.call-update) | async-done | bytes 2097168 | tf_op jit(solution)/shard_map/all_gather | solution.py:31
  74.2 2.6 fusion.7
  76.8 47.2 %all-gather.13.cloned.1.call-done = bf16[2048,512]{1,0:T(8,128)(2,1)} async-done(((bf16[256,512]{1,0:T(8,128)(2,1)}), bf16[2048,512]{1,0:T(8,128)(2,1)}) %all-gather.13.cloned.1.call-update) | async-done | bytes 2097168 | tf_op jit(solution)/shard_map/all_gather | solution.py:33
  123.9 0.0 copy-done.2
  124.0 2.3 fusion.6
  126.3 47.3 %all-gather.11.cloned.1.call-done = bf16[2048,512]{1,0:T(8,128)(2,1)} async-done(((bf16[256,512]{1,0:T(8,128)(2,1)}), bf16[2048,512]{1,0:T(8,128)(2,1)}) %all-gather.11.cloned.1.call-update) | async-done | bytes 2097168 | tf_op jit(solution)/shard_map/all_gather | solution.py:32
  173.6 50.8 %all-gather.17.cloned.1.call-done = bf16[512,2048]{1,0:T(8,128)(2,1)} async-done(((bf16[512,256]{1,0:T(8,128)(2,1)}), bf16[512,2048]{1,0:T(8,128)(2,1)}) %all-gather.17.cloned.1.call-update) | async-done | bytes 2097168 | tf_op jit(solution)/shard_map/all_gather | solution.py:49
  224.4 0.0 copy-start
  224.4 4.7 convolution_convert_fusion.1
  229.1 0.0 reduce-scatter.3.cloned.1.call-update
  229.1 0.0 all-gather.19.cloned.1.call-start
  229.2 6.7 reduce-scatter.3.cloned.1.call-done
  235.8 0.0 copy-done
  235.9 1.3 fusion.12
  237.2 0.0 copy-done.3
  237.2 2.0 fusion.14
  239.2 0.0 all-gather.19.cloned.1.call-update
  239.2 0.0 all-gather.21.cloned.1.call-start
  239.3 0.7 all-gather.21.cloned.1.call-update
  240.0 0.0 all-gather.23.cloned.1.call-start
  240.0 0.7 all-gather.23.cloned.1.call-update
  240.7 0.0 copy-start.1
  240.7 0.0 reduce-scatter.5.cloned.1.call-start
  240.8 8.9 %all-gather.19.cloned.1.call-done = bf16[256,2048]{1,0:T(8,128)(2,1)} async-done(((bf16[128,2048]{1,0:T(8,128)(2,1)}), bf16[256,2048]{1,0:T(8,128)(2,1)}) %all-gather.19.cloned.1.call-update) | async-done | bytes 1048592 | tf_op jit(solution)/shard_map/all_gather | solution.py:59
  249.6 230.6 %all-gather.21.cloned.1.call-done = bf16[2048,4096]{1,0:T(8,128)(2,1)} async-done(((bf16[256,4096]{1,0:T(8,128)(2,1)}), bf16[2048,4096]{1,0:T(8,128)(2,1)}) %all-gather.21.cloned.1.call-update) | async-done | bytes 16777232 | tf_op jit(solution)/shard_map/all_gather | solution.py:60
  480.2 227.6 %all-gather.23.cloned.1.call-done = bf16[4096,2048]{1,0:T(8,128)(2,1)} async-done(((bf16[4096,256]{1,0:T(8,128)(2,1)}), bf16[4096,2048]{1,0:T(8,128)(2,1)}) %all-gather.23.cloned.1.call-update) | async-done | bytes 16777232 | tf_op jit(solution)/shard_map/all_gather | solution.py:63
  707.8 16.5 %convolution_convert_fusion = bf16[256,2048]{1,0:T(8,128)(2,1)} fusion(bf16[4096,2048]{1,0:T(8,128)(2,1)} %all-gather.23.cloned.1.call-done, bf16[256,2048]{1,0:T(8,128)(2,1)} %all-gather.19.cloned.1.call-done, bf16[2048,4096]{1,0:T(8,128)(2,1)} %all-gather.21.cloned.1.call-done), kind=kOutput, calls=%fused_computation.3 | convolution fusion | flops 8593604608 | bytes 35651584 | tf_op jit(solution)/shard_map/dot_general | solution.py:66
  724.3 0.0 reduce-scatter.5.cloned.1.call-update
  724.4 6.7 reduce-scatter.5.cloned.1.call-done
  731.1 0.0 copy-done.1
  731.1 2.1 fusion.15
  (4 shorter events, 0.0 us)
Async XLA Ops:
  6.5 6.0 copy-start.4
  6.5 15.2 %all-gather.9.cloned.1.call-start = ((), (), s32[]{:S(2)}) async-start(), calls=%async_computation.2 | async-start | bytes 1572864 | tf_op jit(solution)/shard_map/all_gather | solution.py:28
  9.8 64.3 %all-gather.15.cloned.1.call-start = ((), (), s32[]{:S(2)}) async-start(), calls=%async_computation.5 | async-start | bytes 2359296 | tf_op jit(solution)/shard_map/all_gather | solution.py:31
  10.6 113.4 %all-gather.13.cloned.1.call-start = ((), (), s32[]{:S(2)}) async-start(), calls=%async_computation.4 | async-start | bytes 2359296 | tf_op jit(solution)/shard_map/all_gather | solution.py:33
  11.3 162.3 %all-gather.11.cloned.1.call-start = ((), (), s32[]{:S(2)}) async-start(), calls=%async_computation.3 | async-start | bytes 2359296 | tf_op jit(solution)/shard_map/all_gather | solution.py:32
  11.9 212.5 %all-gather.17.cloned.1.call-start = ((), (), s32[]{:S(2)}) async-start(), calls=%async_computation.6 | async-start | bytes 2359296 | tf_op jit(solution)/shard_map/all_gather | solution.py:49
  12.5 223.4 %reduce-scatter.3.cloned.1.call-start = ((), (), s32[]{:S(2)}) async-start(), calls=%async_computation.7 | async-start | bytes 1572864 | tf_op jit(solution)/shard_map/reduce_scatter | solution.py:51
  21.7 102.2 %copy-start.2 = (bf16[256,2048]{1,0:T(8,128)(2,1)S(1)}, bf16[256,2048]{1,0:T(8,128)(2,1)}, u32[]{:S(2)}) copy-start(bf16[256,2048]{1,0:T(8,128)(2,1)} %all-gather.9.cloned.1.call-done) | copy-start | bytes 3145732
  224.4 11.5 %copy-start = (bf16[128,2048]{1,0:T(8,128)(2,1)S(1)}, bf16[128,2048]{1,0:T(8,128)(2,1)}, u32[]{:S(2)}) copy-start(bf16[128,2048]{1,0:T(8,128)(2,1)} %param.10) | copy-start | bytes 1572868
  229.1 8.1 %copy-start.3 = (f32[2048]{0:T(1024)S(1)}, f32[2048]{0:T(1024)}, u32[]{:S(2)}) copy-start(f32[2048]{0:T(1024)} %param.17) | copy-start | bytes 24580
  229.1 20.5 %all-gather.19.cloned.1.call-start = ((), (), s32[]{:S(2)}) async-start(), calls=%async_computation.8 | async-start | bytes 1572864 | tf_op jit(solution)/shard_map/all_gather | solution.py:59
  239.2 241.0 %all-gather.21.cloned.1.call-start = ((), (), s32[]{:S(2)}) async-start(), calls=%async_computation.9 | async-start | bytes 18874368 | tf_op jit(solution)/shard_map/all_gather | solution.py:60
  240.0 467.8 %all-gather.23.cloned.1.call-start = ((), (), s32[]{:S(2)}) async-start(), calls=%async_computation.10 | async-start | bytes 18874368 | tf_op jit(solution)/shard_map/all_gather | solution.py:63
  240.7 490.4 %copy-start.1 = (bf16[128,2048]{1,0:T(8,128)(2,1)S(1)}, bf16[128,2048]{1,0:T(8,128)(2,1)}, u32[]{:S(2)}) copy-start(bf16[128,2048]{1,0:T(8,128)(2,1)} %reduce-scatter.3.cloned.1.call-done) | copy-start | bytes 1572868
  240.7 490.4 %reduce-scatter.5.cloned.1.call-start = ((), (), s32[]{:S(2)}) async-start(), calls=%async_computation.11 | async-start | bytes 1572864 | tf_op jit(solution)/shard_map/reduce_scatter | solution.py:65
Sparse Core Ops, SparseCore 0:
  10.0 11.7 all-gather.8
  23.9 50.2 all-gather.14
  76.3 47.6 all-gather.12
  125.9 47.6 all-gather.10
  175.5 48.8 all-gather.16
  229.2 6.5 reduce-scatter.2
  239.3 10.2 all-gather.18
  251.7 228.4 all-gather.20
  482.3 225.4 all-gather.22
  724.5 6.5 reduce-scatter.4
where the time goes:
time: 740 us
  waiting for transfers between devices  691 us (93%)
  matrix products  26.2 us (4%)
  between operations  13.6 us (2%)
  other arithmetic  8.69 us (1%)
    all_gather x1, waiting for transfers between devices, on_device(): up_full = lax.all_gather(up_weight, 'fs', axis=0, tiled=True)  231 us
    all_gather x1, waiting for transfers between devices, on_device(): down_full = lax.all_gather(down_weight, 'fs', axis=1, tiled=True)  228 us
    all_gather x1, waiting for transfers between devices, on_device(): lax.all_gather(conv_in_weight, 'fs', axis=0, tiled=True)  52.4 us
    all_gather x1, waiting for transfers between devices, on_device(): out_full = lax.all_gather(out_weight, 'fs', axis=1, tiled=True)  50.8 us
    all_gather x1, waiting for transfers between devices, on_device(): lax.all_gather(gate_outer_weight, 'fs', axis=0, tiled=True)  47.3 us
    all_gather x1, waiting for transfers between devices, on_device(): lax.all_gather(gate_inner_weight, 'fs', axis=0, tiled=True)  47.2 us
    dot_general x1, matrix products, on_device(): jnp.dot(lefts, down_full, preferred_element_type=jnp.float32)  16.5 us
  transfers between devices with their start and end apart: 10, of which 10 were waited for; matrix products, arithmetic and copies ran while one was open for 1% of the time, Pallas kernels for 0%

commit v1 on v0

--- a/solution.py
+++ b/solution.py
@@ -46,7 +46,7 @@
         + conv_taps[2] * padded[2 : seq_rows + 2]
     )
     mixed = (gate_outer.astype(jnp.float32) * convolved).astype(jnp.bfloat16)
-    out_full = lax.all_gather(out_weight, "fs", axis=1, tiled=True)
+    out_full = jnp.concatenate(lax.all_gather(out_weight, "fs"), axis=1)
     lefts = mixed
     mix_total = lax.psum_scatter(
         jnp.dot(lefts, out_full, preferred_element_type=jnp.float32).astype(jnp.bfloat16),

time: 740 us -> 738 us (level)
  transfers between devices with their start and end apart: 10 -> 10, of which waited for: 10 -> 10; matrix products, arithmetic and copies ran while one was open for 1% -> 2% of each run, Pallas kernels for 0% -> 0%
where the time goes in v1:
time: 738 us
  waiting for transfers between devices  686 us (93%)
  matrix products  26.1 us (4%)
  between operations  13.6 us (2%)
  other arithmetic  8.69 us (1%)
    all_gather x1, waiting for transfers between devices, on_device(): up_full = lax.all_gather(up_weight, 'fs', axis=0, tiled=True)  231 us
    all_gather x1, waiting for transfers between devices, on_device(): down_full = lax.all_gather(down_weight, 'fs', axis=1, tiled=True)  228 us
    all_gather x1, waiting for transfers between devices, on_device(): lax.all_gather(conv_in_weight, 'fs', axis=0, tiled=True)  52.4 us
    all_gather x1, waiting for transfers between devices, on_device(): out_full = jnp.concatenate(lax.all_gather(out_weight, 'fs'), axis=1)  48.7 us
    all_gather x1, waiting for transfers between devices, on_device(): lax.all_gather(gate_inner_weight, 'fs', axis=0, tiled=True)  47 us
    all_gather x1, waiting for transfers between devices, on_device(): lax.all_gather(gate_outer_weight, 'fs', axis=0, tiled=True)  47 us
    dot_general x1, matrix products, on_device(): jnp.dot(lefts, down_full, preferred_element_type=jnp.float32)  16.5 us
  transfers between devices with their start and end apart: 10, of which 10 were waited for; matrix products, arithmetic and copies ran while one was open for 2% of the time, Pallas kernels for 0%

profile of v1, /device:TPU:0, one launch (start us, length us, event | category | flops | bytes accessed | tf_op | source)
XLA Modules:
  0.0 737.7 jit_solution(13663034521417805884)
XLA Ops:
  6.5 0.0 copy-start.3
  6.5 0.0 all-gather.24.cloned.1.call-start
  6.5 0.7 all-gather.24.cloned.1.call-update
  7.3 0.0 all-gather.10.cloned.1.call-start
  7.3 1.2 fusion.8
  8.5 2.0 fusion.10
  10.6 0.0 all-gather.10.cloned.1.call-update
  10.6 0.0 all-gather.16.cloned.1.call-start
  10.6 0.7 all-gather.16.cloned.1.call-update
  11.3 0.0 all-gather.14.cloned.1.call-start
  11.4 0.5 all-gather.14.cloned.1.call-update
  11.9 0.0 all-gather.12.cloned.1.call-start
  12.0 0.5 all-gather.12.cloned.1.call-update
  12.5 0.0 reduce-scatter.3.cloned.1.call-start
  12.5 0.0 copy-done.3
  12.6 48.7 %all-gather.24.cloned.1.call-done = bf16[4096,256]{1,0:T(8,128)(2,1)} async-done(((bf16[512,256]{1,0:T(8,128)(2,1)}), bf16[4096,256]{1,0:T(8,128)(2,1)}) %all-gather.24.cloned.1.call-update) | async-done | bytes 2097168 | tf_op jit(solution)/shard_map/all_gather | solution.py:49
  61.3 2.9 copy.11
  64.2 6.3 all-gather.10.cloned.1.call-done
  70.4 52.4 %all-gather.16.cloned.1.call-done = bf16[2048,512]{1,0:T(8,128)(2,1)} async-done(((bf16[256,512]{1,0:T(8,128)(2,1)}), bf16[2048,512]{1,0:T(8,128)(2,1)}) %all-gather.16.cloned.1.call-update) | async-done | bytes 2097168 | tf_op jit(solution)/shard_map/all_gather | solution.py:31
  122.9 2.6 fusion.7
  125.5 47.0 %all-gather.14.cloned.1.call-done = bf16[2048,512]{1,0:T(8,128)(2,1)} async-done(((bf16[256,512]{1,0:T(8,128)(2,1)}), bf16[2048,512]{1,0:T(8,128)(2,1)}) %all-gather.14.cloned.1.call-update) | async-done | bytes 2097168 | tf_op jit(solution)/shard_map/all_gather | solution.py:33
  172.5 2.6 fusion.6
  175.1 47.0 %all-gather.12.cloned.1.call-done = bf16[2048,512]{1,0:T(8,128)(2,1)} async-done(((bf16[256,512]{1,0:T(8,128)(2,1)}), bf16[2048,512]{1,0:T(8,128)(2,1)}) %all-gather.12.cloned.1.call-update) | async-done | bytes 2097168 | tf_op jit(solution)/shard_map/all_gather | solution.py:32
  222.1 0.0 copy-start
  222.1 4.3 convolution_convert_fusion.1
  226.4 0.0 copy-start.2
  226.4 0.0 reduce-scatter.3.cloned.1.call-update
  226.5 0.0 all-gather.18.cloned.1.call-start
  226.5 7.0 reduce-scatter.3.cloned.1.call-done
  233.5 0.0 copy-done
  233.5 1.3 fusion.12
  234.8 0.0 copy-done.2
  234.9 2.0 fusion.14
  236.9 0.0 all-gather.18.cloned.1.call-update
  236.9 0.0 all-gather.20.cloned.1.call-start
  237.0 0.7 all-gather.20.cloned.1.call-update
  237.7 0.0 all-gather.22.cloned.1.call-start
  237.7 0.7 all-gather.22.cloned.1.call-update
  238.4 0.0 copy-start.1
  238.4 0.0 reduce-scatter.5.cloned.1.call-start
  238.5 8.9 %all-gather.18.cloned.1.call-done = bf16[256,2048]{1,0:T(8,128)(2,1)} async-done(((bf16[128,2048]{1,0:T(8,128)(2,1)}), bf16[256,2048]{1,0:T(8,128)(2,1)}) %all-gather.18.cloned.1.call-update) | async-done | bytes 1048592 | tf_op jit(solution)/shard_map/all_gather | solution.py:59
  247.3 230.6 %all-gather.20.cloned.1.call-done = bf16[2048,4096]{1,0:T(8,128)(2,1)} async-done(((bf16[256,4096]{1,0:T(8,128)(2,1)}), bf16[2048,4096]{1,0:T(8,128)(2,1)}) %all-gather.20.cloned.1.call-update) | async-done | bytes 16777232 | tf_op jit(solution)/shard_map/all_gather | solution.py:60
  477.9 227.6 %all-gather.22.cloned.1.call-done = bf16[4096,2048]{1,0:T(8,128)(2,1)} async-done(((bf16[4096,256]{1,0:T(8,128)(2,1)}), bf16[4096,2048]{1,0:T(8,128)(2,1)}) %all-gather.22.cloned.1.call-update) | async-done | bytes 16777232 | tf_op jit(solution)/shard_map/all_gather | solution.py:63
  705.5 16.5 %convolution_convert_fusion = bf16[256,2048]{1,0:T(8,128)(2,1)} fusion(bf16[4096,2048]{1,0:T(8,128)(2,1)} %all-gather.22.cloned.1.call-done, bf16[256,2048]{1,0:T(8,128)(2,1)} %all-gather.18.cloned.1.call-done, bf16[2048,4096]{1,0:T(8,128)(2,1)} %all-gather.20.cloned.1.call-done), kind=kOutput, calls=%fused_computation.3 | convolution fusion | flops 8593604608 | bytes 35651584 | tf_op jit(solution)/shard_map/dot_general | solution.py:66
  722.0 0.0 reduce-scatter.5.cloned.1.call-update
  722.1 6.7 reduce-scatter.5.cloned.1.call-done
  728.8 0.0 copy-done.1
  728.8 2.1 fusion.15
  (3 shorter events, 0.0 us)
Async XLA Ops:
  6.5 6.0 copy-start.3
  6.5 54.8 %all-gather.24.cloned.1.call-start = ((), (), s32[]{:S(2)}) async-start(), calls=%async_computation.11 | async-start | bytes 2359296 | tf_op jit(solution)/shard_map/all_gather | solution.py:49
  7.3 63.2 %all-gather.10.cloned.1.call-start = ((), (), s32[]{:S(2)}) async-start(), calls=%async_computation.2 | async-start | bytes 1572864 | tf_op jit(solution)/shard_map/all_gather | solution.py:28
  10.6 112.3 %all-gather.16.cloned.1.call-start = ((), (), s32[]{:S(2)}) async-start(), calls=%async_computation.5 | async-start | bytes 2359296 | tf_op jit(solution)/shard_map/all_gather | solution.py:31
  11.3 161.2 %all-gather.14.cloned.1.call-start = ((), (), s32[]{:S(2)}) async-start(), calls=%async_computation.4 | async-start | bytes 2359296 | tf_op jit(solution)/shard_map/all_gather | solution.py:33
  11.9 210.2 %all-gather.12.cloned.1.call-start = ((), (), s32[]{:S(2)}) async-start(), calls=%async_computation.3 | async-start | bytes 2359296 | tf_op jit(solution)/shard_map/all_gather | solution.py:32
  12.5 221.0 %reduce-scatter.3.cloned.1.call-start = ((), (), s32[]{:S(2)}) async-start(), calls=%async_computation.6 | async-start | bytes 1572864 | tf_op jit(solution)/shard_map/reduce_scatter | solution.py:51
  222.1 11.4 %copy-start = (bf16[128,2048]{1,0:T(8,128)(2,1)S(1)}, bf16[128,2048]{1,0:T(8,128)(2,1)}, u32[]{:S(2)}) copy-start(bf16[128,2048]{1,0:T(8,128)(2,1)} %param.10) | copy-start | bytes 1572868
  226.4 8.4 %copy-start.2 = (f32[2048]{0:T(1024)S(1)}, f32[2048]{0:T(1024)}, u32[]{:S(2)}) copy-start(f32[2048]{0:T(1024)} %param.17) | copy-start | bytes 24580
  226.5 20.9 %all-gather.18.cloned.1.call-start = ((), (), s32[]{:S(2)}) async-start(), calls=%async_computation.7 | async-start | bytes 1572864 | tf_op jit(solution)/shard_map/all_gather | solution.py:59
  236.9 241.0 %all-gather.20.cloned.1.call-start = ((), (), s32[]{:S(2)}) async-start(), calls=%async_computation.8 | async-start | bytes 18874368 | tf_op jit(solution)/shard_map/all_gather | solution.py:60
  237.7 467.8 %all-gather.22.cloned.1.call-start = ((), (), s32[]{:S(2)}) async-start(), calls=%async_computation.9 | async-start | bytes 18874368 | tf_op jit(solution)/shard_map/all_gather | solution.py:63
  238.4 490.4 %copy-start.1 = (bf16[128,2048]{1,0:T(8,128)(2,1)S(1)}, bf16[128,2048]{1,0:T(8,128)(2,1)}, u32[]{:S(2)}) copy-start(bf16[128,2048]{1,0:T(8,128)(2,1)} %reduce-scatter.3.cloned.1.call-done) | copy-start | bytes 1572868
  238.4 490.4 %reduce-scatter.5.cloned.1.call-start = ((), (), s32[]{:S(2)}) async-start(), calls=%async_computation.10 | async-start | bytes 1572864 | tf_op jit(solution)/shard_map/reduce_scatter | solution.py:65
Sparse Core Ops, SparseCore 0:
  9.5 51.7 all-gather.23
  62.8 7.5 all-gather.9
  72.6 50.2 all-gather.15
  124.8 47.6 all-gather.13
  174.5 47.6 all-gather.11
  226.6 6.8 reduce-scatter.2
  237.0 10.2 all-gather.17
  249.5 228.4 all-gather.19
  480.0 225.4 all-gather.21
  722.2 6.5 reduce-scatter.4
